TPU v7x, 128 devices: a whole 4x4x4 slice. The times are simulated.
128 devices in a mesh: sp: 16 (over z, y), fs: 4 (over x), tp: 2 (over core).
Axes of the slice: x: 4, y: 4, z: 4, core: 2. Of those that a mesh axis runs over, the one named last changes fastest.
Arguments:
- attn_query: bfloat16 [4, 4096, 2048], P('fs', 'sp', 'tp'), may hold values from -8 to 8
- attn_key: bfloat16 [4, 4096, 2048], P('fs', 'sp', 'tp'), may hold values from -8 to 8
- attn_value: bfloat16 [4, 4096, 2048], P('fs', 'sp', 'tp'), may hold values from -6 to 6
- head_lambda: float32 [16], P('tp'), may hold values from 0.3 to 0.8
- cell_query: bfloat16 [4, 4096, 1024], P('fs', 'sp', 'tp'), may hold values from -6 to 6
- cell_key: bfloat16 [4, 4096, 1024], P('fs', 'sp', 'tp'), may hold values from -6 to 6
- cell_value: bfloat16 [4, 4096, 2048], P('fs', 'sp', 'tp'), may hold values from -6 to 6
- input_pre: float32 [4, 16, 4096], P('fs', 'tp', 'sp'), may hold values from -5 to 140
- forget_pre: float32 [4, 16, 4096], P('fs', 'tp', 'sp'), may hold values from -2 to 16
- out_attn: bfloat16 [2048, 2048], P('tp', 'fs'), may hold values from -0.09375 to 0.09375
- out_cell: bfloat16 [2048, 2048], P('tp', 'fs'), may hold values from -0.09375 to 0.09375
Outputs:
- layer_out: bfloat16 [4, 4096, 2048], P('fs', ('sp', 'tp'))
All inputs are finite; a program needn't handle non-finite values.
Results may differ from a plain program's by a relative error of at most 0.0095.
Values may be sent and summed in bfloat16 or wider, within the bound.
A program may use at most 128 MiB of HBM per device.

v0:
```python
import math

import jax
import jax.numpy as jnp
from jax import lax
from jax.sharding import PartitionSpec as P

DK = 64
DV = 128
CK = 64
CV = 128


EPS = 1e-06
LAMBDA_INIT = 0.2
NEG = -1e30


def sent_to_all(value, axis):
    copies = jnp.broadcast_to(value, (lax.axis_size(axis), *value.shape))
    return lax.all_to_all(copies, axis, split_axis=0, concat_axis=0, tiled=True)


def in_order(tiles, dim):
    dims = list(tiles.shape[1:])
    dims[dim] *= tiles.shape[0]
    return jnp.moveaxis(tiles, 0, dim).reshape(dims)


def collect(value, axis, dim):
    tiles = sent_to_all(value, axis)
    return in_order(tiles, dim)


def side_by_side(arrays, axis, dim, along):
    columns = [a.reshape(*a.shape[:along], -1) for a in arrays]
    both = jnp.concatenate(columns, axis=along)
    whole, at, done = (lax.all_gather(both, axis, axis=dim, tiled=True), 0, [])
    for a, column in zip(arrays, columns):
        section = whole[..., at : at + column.shape[along]]
        done.append(section.reshape(*section.shape[:along], *a.shape[along:]))
        at += column.shape[along]
    return tuple(done)


def sent_together(arrays, axis, dim, along):
    ends, at = ([], 0)
    for a in arrays[:-1]:
        at += a.shape[along]
        ends.append(at)
    both = jnp.concatenate(arrays, axis=along)
    return tuple(jnp.split(collect(both, axis, dim), ends, axis=along))


def cut_along(value, dim, count):
    dims = value.shape
    tiles = value.reshape(*dims[:dim], count, dims[dim] // count, *dims[dim + 1 :])
    return jnp.moveaxis(tiles, dim, 0)


def summed_on_arrival(value, axis, dim):
    tiles = cut_along(value, dim, lax.axis_size(axis))
    arrived = lax.all_to_all(tiles, axis, split_axis=0, concat_axis=0, tiled=True)
    return arrived.astype(jnp.float32).sum(axis=0)


def head_norm(value_rows, heads):
    rows = value_rows.shape[0]
    grouped = value_rows.reshape(rows, heads, -1)
    factor = lax.rsqrt(jnp.mean(grouped * grouped, axis=-1, keepdims=True) + EPS)
    return (grouped * factor).reshape(rows, -1)


def cell_summary(keys_blk, values_blk, gate_blk, forget_blk):
    cumul = jnp.cumsum(forget_blk, axis=-1)
    totals = cumul[:, -1]
    expo = totals[:, None] - cumul + gate_blk
    local_max = jnp.max(expo, axis=-1)
    scaled = jnp.exp(expo - local_max[:, None])
    weighted = (scaled[:, :, None] * keys_blk).astype(jnp.bfloat16)
    local_state = jnp.einsum(
        "htd,hte->hde", weighted, values_blk, preferred_element_type=jnp.float32
    )
    return (cumul, totals, local_max, local_state)


def cell_output(query_blk, keys_blk, values_blk, gate_blk, cumul, prev_state, prior_stabilizer):
    length = cumul.shape[-1]
    diff = cumul[:, :, None] - cumul[:, None, :] + gate_blk[:, None, :]
    causal = (
        jnp.arange(length, dtype=jnp.int32)[:, None] >= jnp.arange(length, dtype=jnp.int32)[None, :]
    )
    diff = jnp.where(causal[None], diff, NEG)
    inter = cumul + prior_stabilizer[:, None]
    stab = jnp.maximum(jnp.max(diff, axis=-1), inter)
    scores = jnp.einsum(
        "hjd,hkd->hjk", query_blk, keys_blk, preferred_element_type=jnp.float32
    ) * CK ** (-0.5)
    probs = (jnp.exp(diff - stab[..., None]) * scores).astype(jnp.bfloat16)
    intra = jnp.einsum("hjk,hke->hje", probs, values_blk, preferred_element_type=jnp.float32)
    carried = jnp.einsum(
        "hjd,hde->hje", query_blk.astype(jnp.float32), prev_state, precision=lax.Precision.HIGHEST
    ) * CK ** (-0.5)
    return intra + jnp.exp(inter - stab)[..., None] * carried


def per_device(
    attn_query,
    attn_key,
    attn_value,
    head_lambda,
    cell_query,
    cell_key,
    cell_value,
    input_pre,
    forget_pre,
    out_attn,
    out_cell,
):
    tokens = attn_query.shape[1]
    heads_attn = head_lambda.shape[0]
    heads_cell = input_pre.shape[1]
    position = lax.axis_index("sp")
    length_sp = lax.axis_size("sp")
    query_pos = position * tokens + jnp.arange(tokens, dtype=jnp.int32)
    last_pos = position * tokens + tokens - 1
    query_cell = cell_query[0].reshape(tokens, heads_cell, CK).transpose(1, 0, 2)
    keys_cell = cell_key[0].reshape(tokens, heads_cell, CK).transpose(1, 0, 2)
    values_cell = cell_value[0].reshape(tokens, heads_cell, CV).transpose(1, 0, 2)
    in_gate = input_pre[0]
    log_forget = jax.nn.log_sigmoid(forget_pre[0])
    cumul, totals, local_max, local_state = cell_summary(
        keys_cell, values_cell, in_gate, log_forget
    )
    all_totals = collect(totals[None], "sp", 0)
    inclusive = jnp.cumsum(all_totals, axis=0)
    earlier = jnp.arange(length_sp, dtype=jnp.int32)[:, None] < position
    before = jnp.sum(jnp.where(earlier, all_totals, 0.0), axis=0)
    state_run = jnp.zeros_like(local_state)
    piece_max, piece_state = side_by_side((local_max[None], local_state[None]), "sp", 0, 2)
    shards = piece_max.shape[0]
    indices = jnp.arange(shards, dtype=jnp.int32)
    expo = jnp.where((indices < position)[:, None], before[None, :] - inclusive + piece_max, NEG)
    new_stab = jnp.maximum(before, jnp.max(expo, axis=0))
    weights = jnp.exp(expo - new_stab[None, :])
    state_new = jnp.exp(before - new_stab)[:, None, None] * state_run + jnp.sum(
        weights[:, :, None, None] * piece_state, axis=0
    )
    cell_hidden = cell_output(
        query_cell, keys_cell, values_cell, in_gate, cumul, state_new, new_stab
    )
    cell_out = head_norm(
        cell_hidden.transpose(1, 0, 2).reshape(tokens, heads_cell * CV), heads_cell
    ).astype(jnp.bfloat16)
    query_attn = attn_query[0].reshape(tokens, heads_attn, 2, DK)
    score_scale = DK ** (-0.5)
    start_state = (
        jnp.full((heads_attn, 2, tokens), NEG, jnp.float32),
        jnp.zeros((heads_attn, 2, tokens), jnp.float32),
        jnp.zeros((heads_attn, 2, tokens, DV), jnp.float32),
    )
    keys_piece = lax.all_gather(attn_key, "sp", axis=0, tiled=True)
    values_piece = lax.all_gather(attn_value, "sp", axis=0, tiled=True)
    shards = keys_piece.shape[0]
    group = math.gcd(shards, max(1, 1024 // tokens))
    rounds = shards // group
    keys_grouped = keys_piece.reshape(rounds, group * tokens, heads_attn, 2, DK)
    values_grouped = values_piece.reshape(rounds, group * tokens, heads_attn, DV)

    def one_round(running, pieces):
        keys_blk, values_blk, number = pieces
        first = number * group * tokens

        def update(state):
            row_max, row_total, numerator = state
            scores = (
                jnp.einsum(
                    "qhcd,khcd->hcqk", query_attn, keys_blk, preferred_element_type=jnp.float32
                )
                * score_scale
            )
            key_pos = first + jnp.arange(group * tokens, dtype=jnp.int32)
            scores = jnp.where(key_pos[None, :] <= query_pos[:, None], scores, NEG)
            new_max = jnp.maximum(row_max, jnp.max(scores, axis=-1))
            expd = jnp.exp(scores - new_max[..., None])
            shrink = jnp.exp(row_max - new_max)
            new_total = shrink * row_total + jnp.sum(expd, axis=-1)
            new_numerator = shrink[..., None] * numerator + jnp.einsum(
                "hcqk,khd->hcqd",
                expd.astype(jnp.bfloat16),
                values_blk,
                preferred_element_type=jnp.float32,
            )
            return (new_max, new_total, new_numerator)

        def unchanged(state):
            return state

        return (lax.cond(first <= last_pos, update, unchanged, running), None)

    result, _ = lax.scan(
        one_round, start_state, (keys_grouped, values_grouped, jnp.arange(rounds, dtype=jnp.int32))
    )
    row_max, row_total, numerator = result
    ratio = numerator / row_total[..., None]
    mixed = ratio[:, 0] - head_lambda[:, None, None] * ratio[:, 1]
    mixed = jnp.transpose(mixed, (1, 0, 2)).reshape(tokens, heads_attn * DV)
    attn_out = (head_norm(mixed, heads_attn) * (1.0 - LAMBDA_INIT)).astype(jnp.bfloat16)
    weight_attn, weight_cell = sent_together((out_attn, out_cell), "fs", 1, 0)
    summed = summed_on_arrival(
        (
            jnp.dot(attn_out, weight_attn, preferred_element_type=jnp.float32)
            + jnp.dot(cell_out, weight_cell, preferred_element_type=jnp.float32)
        ).astype(jnp.bfloat16),
        "tp",
        0,
    )
    return summed.astype(jnp.bfloat16)[None]


def solution(mesh):
    placed = (
        P("fs", "sp", "tp"),
        P("fs", "sp", "tp"),
        P("fs", "sp", "tp"),
        P("tp"),
        P("fs", "sp", "tp"),
        P("fs", "sp", "tp"),
        P("fs", "sp", "tp"),
        P("fs", "tp", "sp"),
        P("fs", "tp", "sp"),
        P("tp", "fs"),
        P("tp", "fs"),
    )
    return jax.shard_map(
        per_device,
        mesh=mesh,
        in_specs=placed,
        out_specs=P("fs", ("sp", "tp"), None),
        check_vma=False,
    )
```

profile of v0, /device:TPU:97, one launch (start us, length us, event | category | flops | bytes accessed | tf_op | source)
XLA Modules:
  0.0 377.9 jit_solution(4973251549206276978)
XLA Ops:
  6.5 1.3 copy.70
  7.9 1.1 copy.54
  9.0 0.7 fusion.42
  10.7 0.9 fusion.48
  11.6 0.8 subtract_exponential_fusion.3
  12.8 0.8 pad_maximum_fusion.1
  13.7 0.7 all-gather.4.cloned.1.call-update
  15.8 6.6 %all-to-all-start.1 = ((f32[16,1,8]{2,1,0:T(1,128)}), f32[16,1,8]{2,1,0:T(1,128)S(1)}, u32[]{:S(2)}, u32[]{:S(2)}) async-start(f32[16,1,8]{2,1,0:T(1,128)} %broadcast_in_dim.94), calls=%async_computation.1 | async-start | bytes 16384 | tf_op jit(solution)/shard_map/all_to_all | solution.py:21
  22.4 2.7 pad_maximum_fusion
  25.1 3.0 copy.50
  28.1 4.3 %broadcast_in_dim.90 = bf16[4,2048,512]{1,2,0:T(8,128)(2,1)} broadcast(bf16[2048,512]{0,1:T(8,128)(2,1)S(1)} %copy.50), dimensions={1,2} | broadcast | bytes 10485760 | tf_op jit(solution)/shard_map/broadcast_in_dim | solution.py:20
  32.4 5.9 %all-to-all-start = ((bf16[4,2048,512]{1,2,0:T(8,128)(2,1)}), bf16[4,2048,512]{1,2,0:T(8,128)(2,1)}, u32[]{:S(2)}, u32[]{:S(2)}) async-start(bf16[4,2048,512]{1,2,0:T(8,128)(2,1)} %broadcast_in_dim.90), calls=%async_computation | async-start | bytes 16777216 | tf_op jit(solution)/shard_map/all_to_all | solution.py:21
  39.5 91.3 %all-to-all-done = bf16[4,2048,512]{1,2,0:T(8,128)(2,1)} async-done(((bf16[4,2048,512]{1,2,0:T(8,128)(2,1)}), bf16[4,2048,512]{1,2,0:T(8,128)(2,1)}, u32[]{:S(2)}, u32[]{:S(2)}) %all-to-all-start) | async-done | bytes 8388640 | tf_op jit(solution)/shard_map/all_to_all | solution.py:21
  130.8 5.9 %fusion.52 = (bf16[1024,4,512]{0,2,1:T(8,128)(2,1)}, bf16[1024,4,512]{0,2,1:T(8,128)(2,1)}) fusion(bf16[2048,4,512]{0,2,1:T(8,128)(2,1)} %bitcast.10), kind=kLoop, calls=%fused_computation.87 | loop fusion | bytes 16777216 | tf_op jit(solution)/shard_map/split | solution.py:52
  136.7 0.8 slice.34
  137.9 3.4 fusion.21
  141.3 2.6 copy.71
  143.9 2.8 copy.62
  146.8 1.1 fusion.25
  147.9 0.9 multiply_reduce_fusion
  148.8 0.9 multiply_convert_fusion.1
  149.7 30.0 %reshape.271 = bf16[4,1024,8,2,64]{4,3,2,1,0:T(2,128)(2,1)} reshape(bf16[16,256,1024]{2,1,0:T(8,128)(2,1)} %all-gather.4.cloned.1.call-done) | data formatting | bytes 16777216 | tf_op jit(solution)/shard_map/reshape | solution.py:167
  179.7 39.2 %copy.46 = bf16[4,1024,8,2,64]{1,4,3,2,0:T(8,128)(2,1)} copy(bf16[4,1024,8,2,64]{4,3,2,1,0:T(2,128)(2,1)} %reshape.271) | data formatting | bytes 16777216
  218.9 8.8 %copy.74 = bf16[512,8,8,128]{3,2,1,0:T(8,128)(2,1)} copy(bf16[512,8,8,128]{3,1,2,0:T(8,128)(2,1)} %bitcast.140) | data formatting | bytes 16777216
  227.7 8.6 %copy.47 = bf16[4,1024,8,128]{3,1,2,0:T(8,128)(2,1)} copy(bf16[4,1024,8,128]{3,2,1,0:T(8,128)(2,1)} %bitcast.138) | data formatting | bytes 16777216
  236.5 119.6 %while.17 = (s32[]{:T(128)}, f32[8,2,256]{2,1,0:T(2,128)S(1)}, f32[8,2,256]{2,1,0:T(2,128)S(1)}, f32[8,2,256,128]{3,2,1,0:T(8,128)S(1)}, s32[4]{0:T(128)S(1)}, /...) while((s32[]{:T(128)}, f32[8,2,256]{2,1,0:T(2,128)S(1)}, ...), condition=%wide.region_5.6_spmd.clone, body=%wide.region_0.5_spmd.clone.sunk | while | flops 1658070272 | bytes 60568880 | solution.py:201
  238.1 28.5 %conditional.3 = ((f32[8,2,256]{2,1,0:T(2,128)S(1)}, f32[8,2,256]{2,1,0:T(2,128)S(1)}, f32[8,2,256,128]{3,2,1,0:T(8,128)S(1)})) conditional(s32[]{:T(128)} %convert_element_type.64, (f32[8,2,256]{2,1,0:T(2,128)S(1)}, f32[8,2,256]{2,1,0:T(2,128)S(1)}, f32[8,2,256,128]{3,2,1,0:T(8,128)S(1)}) %tuple.55, (s32[]{:T(128)}, s32[]{:T(128)}, ...), branch_computations={%region_1.1_spmd, %region_2.4_spmd} | conditional | flops 1658070272 | bytes 60567592 | solution.py:199
  238.3 10.0 %fusion.4 = (f32[8,2,256]{2,1,0:T(2,128)S(1)}, f32[8,2,1024,256]{3,2,1,0:T(8,128)}) fusion(pred[256,1024]{0,1:T(8,128)(4,1)S(1)} %broadcast_compare_fusion, bf16[256,8,2,64]{0,3,2,1:T(8,128)(2,1)S(1)} %get-tuple-element.200, bf16[4,1024,8,2,64]{1,4,3,2,0:T(8,128)(2,1)} %get-tuple-element.198, s32[]{:T(128)} %get-tuple-element.199), kind=kOutput, calls=%fused_computation.5 | convolution fusion | flops 549449728 | bytes 19677696 | tf_op jit(solution)/shard_map/while/body/eval_jaxpr/cond/branch_1_fun/qhcd,khcd->hcqk/dot_general | solution.py:177
  248.4 9.2 %fusion.3 = f32[8,2,256]{2,1,0:T(2,128)S(1)} fusion(f32[8,2,1024,256]{3,2,1,0:T(8,128)} %get-tuple-element.296, f32[8,2,256]{2,1,0:T(2,128)S(1)} %max.36, pred[256,1024]{0,1:T(8,128)(4,1)S(1)} %broadcast_compare_fusion), kind=kLoop, calls=%fused_computation.4 | loop fusion | flops 16773120 | bytes 17072128 | tf_op jit(solution)/shard_map/while/body/eval_jaxpr/cond/branch_1_fun/reduce_sum | solution.py:187
  257.6 8.9 %multiply_add_fusion = f32[8,2,256,128]{3,2,1,0:T(8,128)S(1)} fusion(f32[8,2,256,128]{3,2,1,0:T(8,128)S(1)} %get-tuple-element.202, bf16[4,1024,8,128]{3,1,2,0:T(8,128)(2,1)} %get-tuple-element.203, s32[]{:T(128)} %get-tuple-element.199, f32[8,2,1024,256]{3,2,1,0:T(8,128)} %get-tuple-element.296, f32[8,2,256]{2,1,0:T(2,128)S(1)} %max.36, ...), kind=kOutput, calls=%fused_computation.12 | convolution fusion | flops 1091567616 | bytes 23364096 | tf_op jit(solution)/shard_map/while/body/eval_jaxpr/cond/branch_1_fun/hcqk,khd->hcqd/dot_general | solution.py:188
  267.9 28.5 %conditional.3 = ((f32[8,2,256]{2,1,0:T(2,128)S(1)}, f32[8,2,256]{2,1,0:T(2,128)S(1)}, f32[8,2,256,128]{3,2,1,0:T(8,128)S(1)})) conditional(s32[]{:T(128)} %convert_element_type.64, (f32[8,2,256]{2,1,0:T(2,128)S(1)}, f32[8,2,256]{2,1,0:T(2,128)S(1)}, f32[8,2,256,128]{3,2,1,0:T(8,128)S(1)}) %tuple.55, (s32[]{:T(128)}, s32[]{:T(128)}, ...), branch_computations={%region_1.1_spmd, %region_2.4_spmd} | conditional | flops 1658070272 | bytes 60567592 | solution.py:199
  268.2 10.0 %fusion.4 = (f32[8,2,256]{2,1,0:T(2,128)S(1)}, f32[8,2,1024,256]{3,2,1,0:T(8,128)}) fusion(pred[256,1024]{0,1:T(8,128)(4,1)S(1)} %broadcast_compare_fusion, bf16[256,8,2,64]{0,3,2,1:T(8,128)(2,1)S(1)} %get-tuple-element.200, bf16[4,1024,8,2,64]{1,4,3,2,0:T(8,128)(2,1)} %get-tuple-element.198, s32[]{:T(128)} %get-tuple-element.199), kind=kOutput, calls=%fused_computation.5 | convolution fusion | flops 549449728 | bytes 19677696 | tf_op jit(solution)/shard_map/while/body/eval_jaxpr/cond/branch_1_fun/qhcd,khcd->hcqk/dot_general | solution.py:177
  278.2 9.2 %fusion.3 = f32[8,2,256]{2,1,0:T(2,128)S(1)} fusion(f32[8,2,1024,256]{3,2,1,0:T(8,128)} %get-tuple-element.296, f32[8,2,256]{2,1,0:T(2,128)S(1)} %max.36, pred[256,1024]{0,1:T(8,128)(4,1)S(1)} %broadcast_compare_fusion), kind=kLoop, calls=%fused_computation.4 | loop fusion | flops 16773120 | bytes 17072128 | tf_op jit(solution)/shard_map/while/body/eval_jaxpr/cond/branch_1_fun/reduce_sum | solution.py:187
  287.5 8.9 %multiply_add_fusion = f32[8,2,256,128]{3,2,1,0:T(8,128)S(1)} fusion(f32[8,2,256,128]{3,2,1,0:T(8,128)S(1)} %get-tuple-element.202, bf16[4,1024,8,128]{3,1,2,0:T(8,128)(2,1)} %get-tuple-element.203, s32[]{:T(128)} %get-tuple-element.199, f32[8,2,1024,256]{3,2,1,0:T(8,128)} %get-tuple-element.296, f32[8,2,256]{2,1,0:T(2,128)S(1)} %max.36, ...), kind=kOutput, calls=%fused_computation.12 | convolution fusion | flops 1091567616 | bytes 23364096 | tf_op jit(solution)/shard_map/while/body/eval_jaxpr/cond/branch_1_fun/hcqk,khd->hcqd/dot_general | solution.py:188
  297.8 28.5 %conditional.3 = ((f32[8,2,256]{2,1,0:T(2,128)S(1)}, f32[8,2,256]{2,1,0:T(2,128)S(1)}, f32[8,2,256,128]{3,2,1,0:T(8,128)S(1)})) conditional(s32[]{:T(128)} %convert_element_type.64, (f32[8,2,256]{2,1,0:T(2,128)S(1)}, f32[8,2,256]{2,1,0:T(2,128)S(1)}, f32[8,2,256,128]{3,2,1,0:T(8,128)S(1)}) %tuple.55, (s32[]{:T(128)}, s32[]{:T(128)}, ...), branch_computations={%region_1.1_spmd, %region_2.4_spmd} | conditional | flops 1658070272 | bytes 60567592 | solution.py:199
  298.0 10.0 %fusion.4 = (f32[8,2,256]{2,1,0:T(2,128)S(1)}, f32[8,2,1024,256]{3,2,1,0:T(8,128)}) fusion(pred[256,1024]{0,1:T(8,128)(4,1)S(1)} %broadcast_compare_fusion, bf16[256,8,2,64]{0,3,2,1:T(8,128)(2,1)S(1)} %get-tuple-element.200, bf16[4,1024,8,2,64]{1,4,3,2,0:T(8,128)(2,1)} %get-tuple-element.198, s32[]{:T(128)} %get-tuple-element.199), kind=kOutput, calls=%fused_computation.5 | convolution fusion | flops 549449728 | bytes 19677696 | tf_op jit(solution)/shard_map/while/body/eval_jaxpr/cond/branch_1_fun/qhcd,khcd->hcqk/dot_general | solution.py:177
  308.1 9.2 %fusion.3 = f32[8,2,256]{2,1,0:T(2,128)S(1)} fusion(f32[8,2,1024,256]{3,2,1,0:T(8,128)} %get-tuple-element.296, f32[8,2,256]{2,1,0:T(2,128)S(1)} %max.36, pred[256,1024]{0,1:T(8,128)(4,1)S(1)} %broadcast_compare_fusion), kind=kLoop, calls=%fused_computation.4 | loop fusion | flops 16773120 | bytes 17072128 | tf_op jit(solution)/shard_map/while/body/eval_jaxpr/cond/branch_1_fun/reduce_sum | solution.py:187
  317.3 8.9 %multiply_add_fusion = f32[8,2,256,128]{3,2,1,0:T(8,128)S(1)} fusion(f32[8,2,256,128]{3,2,1,0:T(8,128)S(1)} %get-tuple-element.202, bf16[4,1024,8,128]{3,1,2,0:T(8,128)(2,1)} %get-tuple-element.203, s32[]{:T(128)} %get-tuple-element.199, f32[8,2,1024,256]{3,2,1,0:T(8,128)} %get-tuple-element.296, f32[8,2,256]{2,1,0:T(2,128)S(1)} %max.36, ...), kind=kOutput, calls=%fused_computation.12 | convolution fusion | flops 1091567616 | bytes 23364096 | tf_op jit(solution)/shard_map/while/body/eval_jaxpr/cond/branch_1_fun/hcqk,khd->hcqd/dot_general | solution.py:188
  327.6 28.5 %conditional.3 = ((f32[8,2,256]{2,1,0:T(2,128)S(1)}, f32[8,2,256]{2,1,0:T(2,128)S(1)}, f32[8,2,256,128]{3,2,1,0:T(8,128)S(1)})) conditional(s32[]{:T(128)} %convert_element_type.64, (f32[8,2,256]{2,1,0:T(2,128)S(1)}, f32[8,2,256]{2,1,0:T(2,128)S(1)}, f32[8,2,256,128]{3,2,1,0:T(8,128)S(1)}) %tuple.55, (s32[]{:T(128)}, s32[]{:T(128)}, ...), branch_computations={%region_1.1_spmd, %region_2.4_spmd} | conditional | flops 1658070272 | bytes 60567592 | solution.py:199
  327.9 10.0 %fusion.4 = (f32[8,2,256]{2,1,0:T(2,128)S(1)}, f32[8,2,1024,256]{3,2,1,0:T(8,128)}) fusion(pred[256,1024]{0,1:T(8,128)(4,1)S(1)} %broadcast_compare_fusion, bf16[256,8,2,64]{0,3,2,1:T(8,128)(2,1)S(1)} %get-tuple-element.200, bf16[4,1024,8,2,64]{1,4,3,2,0:T(8,128)(2,1)} %get-tuple-element.198, s32[]{:T(128)} %get-tuple-element.199), kind=kOutput, calls=%fused_computation.5 | convolution fusion | flops 549449728 | bytes 19677696 | tf_op jit(solution)/shard_map/while/body/eval_jaxpr/cond/branch_1_fun/qhcd,khcd->hcqk/dot_general | solution.py:177
  337.9 9.2 %fusion.3 = f32[8,2,256]{2,1,0:T(2,128)S(1)} fusion(f32[8,2,1024,256]{3,2,1,0:T(8,128)} %get-tuple-element.296, f32[8,2,256]{2,1,0:T(2,128)S(1)} %max.36, pred[256,1024]{0,1:T(8,128)(4,1)S(1)} %broadcast_compare_fusion), kind=kLoop, calls=%fused_computation.4 | loop fusion | flops 16773120 | bytes 17072128 | tf_op jit(solution)/shard_map/while/body/eval_jaxpr/cond/branch_1_fun/reduce_sum | solution.py:187
  347.2 8.9 %multiply_add_fusion = f32[8,2,256,128]{3,2,1,0:T(8,128)S(1)} fusion(f32[8,2,256,128]{3,2,1,0:T(8,128)S(1)} %get-tuple-element.202, bf16[4,1024,8,128]{3,1,2,0:T(8,128)(2,1)} %get-tuple-element.203, s32[]{:T(128)} %get-tuple-element.199, f32[8,2,1024,256]{3,2,1,0:T(8,128)} %get-tuple-element.296, f32[8,2,256]{2,1,0:T(2,128)S(1)} %max.36, ...), kind=kOutput, calls=%fused_computation.12 | convolution fusion | flops 1091567616 | bytes 23364096 | tf_op jit(solution)/shard_map/while/body/eval_jaxpr/cond/branch_1_fun/hcqk,khd->hcqd/dot_general | solution.py:188
  356.1 1.9 copy.49
  358.0 1.9 broadcast_divide_fusion
  360.9 1.3 fusion.53
  362.6 1.3 fusion.22
  363.9 6.3 %all_to_all.15 = bf16[2,128,2048]{2,1,0:T(8,128)(2,1)S(1)} all-to-all(bf16[2,128,2048]{2,1,0:T(8,128)(2,1)S(1)} %bitcast.150), channel_id=1, replica_groups=mesh['sp'=16,'fs'=4,'tp'=2] {'tp'}, dimensions={0} | all-to-all | bytes 2097152 | tf_op jit(solution)/shard_map/all_to_all | solution.py:63
  370.3 1.1 reduce_sum.66
  (88 shorter events, 9.5 us)
Async XLA Ops:
  6.5 15.9 %copy-start.2 = (bf16[1024,512]{1,0:T(8,128)(2,1)S(1)}, bf16[1024,512]{1,0:T(8,128)(2,1)}, u32[]{:S(2)}) copy-start(bf16[1024,512]{1,0:T(8,128)(2,1)} %param.25) | copy-start | bytes 3145732
  6.5 130.2 %all-gather.8.cloned.1.call-start = ((), (), s32[]{:S(2)}) async-start(), calls=%async_computation.5 | async-start | bytes 4526080 | tf_op jit(solution)/shard_map/all_gather | solution.py:38
  13.7 136.0 %all-gather.4.cloned.1.call-start = ((), (), s32[]{:S(2)}) async-start(), calls=%async_computation.3 | async-start | bytes 8912896 | tf_op jit(solution)/shard_map/all_gather | solution.py:162
  14.5 204.4 %all-gather.6.cloned.1.call-start = ((), (), s32[]{:S(2)}) async-start(), calls=%async_computation.4 | async-start | bytes 8912896 | tf_op jit(solution)/shard_map/all_gather | solution.py:163
  15.8 12.3 %all-to-all-start.1 = ((f32[16,1,8]{2,1,0:T(1,128)}), f32[16,1,8]{2,1,0:T(1,128)S(1)}, u32[]{:S(2)}, u32[]{:S(2)}) async-start(f32[16,1,8]{2,1,0:T(1,128)} %broadcast_in_dim.94), calls=%async_computation.1 | async-start | bytes 16384 | tf_op jit(solution)/shard_map/all_to_all | solution.py:21
  32.4 6.0 %copy-start.4 = (bf16[1,256,1024]{2,1,0:T(8,128)(2,1)S(1)}, bf16[1,256,1024]{2,1,0:T(8,128)(2,1)}, u32[]{:S(2)}) copy-start(bf16[1,256,1024]{2,1,0:T(8,128)(2,1)} %param.15) | copy-start | bytes 1572868
  32.4 6.2 %copy-start.5 = (bf16[1,256,512]{2,1,0:T(8,128)(2,1)S(1)}, bf16[1,256,512]{2,1,0:T(8,128)(2,1)}, u32[]{:S(2)}) copy-start(bf16[1,256,512]{2,1,0:T(8,128)(2,1)} %param.19) | copy-start | bytes 786436
  32.4 6.4 %copy-start.6 = (f32[1,8,256]{2,1,0:T(8,128)S(1)}, f32[1,8,256]{2,1,0:T(8,128)}, u32[]{:S(2)}) copy-start(f32[1,8,256]{2,1,0:T(8,128)} %param.22) | copy-start | bytes 24580
  32.4 98.4 %all-to-all-start = ((bf16[4,2048,512]{1,2,0:T(8,128)(2,1)}), bf16[4,2048,512]{1,2,0:T(8,128)(2,1)}, u32[]{:S(2)}, u32[]{:S(2)}) async-start(bf16[4,2048,512]{1,2,0:T(8,128)(2,1)} %broadcast_in_dim.90), calls=%async_computation | async-start | bytes 16777216 | tf_op jit(solution)/shard_map/all_to_all | solution.py:21
  356.1 3.8 %copy-start.7 = (f32[8]{0:T(128)S(1)}, f32[8]{0:T(128)}, u32[]{:S(2)}) copy-start(f32[8]{0:T(128)} %param.18) | copy-start | bytes 100
  358.0 2.8 copy-start.1
  360.2 2.3 copy-start
  360.2 2.4 copy-start.3
Sparse Core Ops, SparseCore 0:
  13.8 52.7 all-gather.7
  68.7 70.5 all-gather.3
  141.4 70.5 all-gather.5
where the time goes:
time: 381 us; the launch traced here: 378 us
  local copies, waits for them, and re-layouts  115 us (30%)
  waiting for transfers between devices  92.7 us (24%)
  matrix products  80.8 us (21%)
  other arithmetic  53.3 us (14%)
  between operations  13.4 us (4%)
  starting transfers between devices  12.6 us (3%)
  blocking collectives  6.34 us (2%)
    all_to_all x2, waiting for transfers between devices, sent_to_all(): return lax.all_to_all(copies, axis, split_axis=0, concat_axis=0, tiled=True)  91.3 us
    unnamed x23, local copies, waits for them, and re-layouts  61.4 us
    dot_general x4, matrix products, update(): jnp.einsum('qhcd,khcd->hcqk', query_attn, keys_blk, preferred_element_typ...  40.2 us
    reduce_sum x4, other arithmetic, update(): new_total = shrink * row_total + jnp.sum(expd, axis=-1)  36.8 us
    dot_general x4, matrix products, update(): jnp.einsum('hcqk,khd->hcqd', expd.astype(jnp.bfloat16), values_blk, prefe...  35.7 us
    reshape x1, local copies, waits for them, and re-layouts, per_device(): keys_grouped = keys_piece.reshape(rounds, group * tokens, heads_attn, 2, DK)  30 us
    all_to_all x2, starting transfers between devices, sent_to_all(): return lax.all_to_all(copies, axis, split_axis=0, concat_axis=0, tiled=True)  12.5 us
  transfers between devices with their start and end apart: 5, of which 1 were waited for; matrix products, arithmetic and copies ran while one was open for 26% of the time, Pallas kernels for 0%

commit v1 on v0

v1 whole, which is shorter than its diff:
```python
import functools

import jax
import jax.numpy as jnp
from jax import lax
from jax.experimental import pallas as pl
from jax.experimental.pallas import tpu as pltpu
from jax.sharding import PartitionSpec as P

MESH = pl.DeviceIdType.MESH
F32 = jnp.float32
BF16 = jnp.bfloat16
NEG = -1e30
EPS = 1e-6

TOK = 256
NSP = 16
NFS = 4
HEADS = 8
DV = 128


def dot_nn(a, b):
    return jnp.dot(a, b, preferred_element_type=F32)


def dot_nt(a, b):
    return lax.dot_general(a, b, (((1,), (1,)), ((), ())), preferred_element_type=F32)


def iota(shape, dim):
    return lax.broadcasted_iota(jnp.int32, shape, dim)


def log_sigmoid(x):
    small = jnp.exp(-jnp.abs(x))
    series = small * (1.0 - small * (0.5 - small * (1.0 / 3.0 - small * 0.25)))
    return jnp.minimum(x, 0.0) - jnp.where(small < 0.01, series, jnp.log(1.0 + small))


def scan_lanes(x, combine, start):
    lane = iota(x.shape, 1)
    shift = 1
    while shift < x.shape[1]:
        moved = pltpu.roll(x, shift, 1)
        x = combine(x, jnp.where(lane >= shift, moved, start))
        shift *= 2
    return x


def kernel(
    aq, ak, av, lam, cq, ck, cv, gi, gf, wa, wc, out,
    kb, vb, vt, qb, sbuf, mx, ls, acc, aout, acta, actc, w, part, own, got,
    cqs, cks, cvs, intra, cvt, hdr, st_out, st_in, pv_out, pv_in, cum_s, u_s, m_s, lamt,
    k_s, v_s, q_s, k_r, v_r, q_r, rk_s, rv_s, as_, ar, w_s, w_r, p_s, p_r,
    st_s, st_r, pv_s, pv_r, c_r, l_s, l_r,
):
    p = lax.axis_index("sp")
    f = lax.axis_index("fs")
    t = lax.axis_index("tp")
    left, right, across = lax.rem(f + 3, NFS), lax.rem(f + 1, NFS), lax.rem(f + 2, NFS)
    owner = lax.rem((p + 1) // 2, 2)
    group = p // HEADS
    row = lax.rem(p, HEADS)

    def remote(src, dst, send, recv, device):
        return pltpu.make_async_remote_copy(
            src_ref=src, dst_ref=dst, send_sem=send, recv_sem=recv, device_id=device, device_id_type=MESH
        )

    def arrived(dst, recv):
        remote(dst, dst, recv, recv, (p, f, 1 - t)).wait_recv()

    def sent(src, send):
        remote(src, src, send, send, (p, f, 1 - t)).wait_send()

    def kv_at(ref, b):
        return ref.at[b // 2, pl.ds(pl.multiple_of(lax.rem(b, 2) * TOK, TOK), TOK), :]

    def cols(i):
        return pl.ds(pl.multiple_of(i * 128, 128), 128)

    barrier = pltpu.get_barrier_semaphore()

    def greet(i, _):
        peer = lax.rem(p * 2 + t + i, 2 * NSP)
        pl.semaphore_signal(barrier, inc=1, device_id=(peer // 2, f, lax.rem(peer, 2)), device_id_type=MESH)
        return 0

    lax.fori_loop(1, 2 * NSP, greet, 0)
    for side in (left, right):
        pl.semaphore_signal(barrier, inc=1, device_id=(p, side, t), device_id_type=MESH)
    pl.semaphore_wait(barrier, 2 * NSP + 1)

    locals_ = (
        (cq, cqs, c_r.at[0]), (ck, cks, c_r.at[1]), (cv, cvs, c_r.at[2]),
        (wa, w.at[f, 0], w_r.at[0, 0]), (wc, w.at[f, 1], w_r.at[0, 1]),
    )
    for src, dst, sem in locals_:
        pltpu.make_async_copy(src, dst, sem).start()

    def send_heads(i, _):
        j = lax.rem(row + i, HEADS)
        h = HEADS * t + j
        here = jnp.logical_and(h == p, t == owner)
        trips = (
            (ak, kv_at(kb, p), k_s, k_r.at[p]),
            (av, kv_at(vb, p), v_s, v_r.at[p]),
            (aq, qb.at[p // 2], q_s, q_r.at[p // 2]),
        )
        for src, dst, send, recv in trips:

            @pl.when(jnp.logical_not(here))
            def _():
                remote(src.at[:, cols(j)], dst, send.at[j], recv, (h, f, owner)).start()

            @pl.when(here)
            def _():
                pltpu.make_async_copy(src.at[:, cols(j)], dst, recv).start()

        return 0

    lax.fori_loop(0, HEADS, send_heads, 0)

    to_right = [remote(x, w.at[f, i], w_s.at[i], w_r.at[1, i], (p, right, t)) for i, x in enumerate((wa, wc))]
    to_left = [remote(x, w.at[f, i], w_s.at[2 + i], w_r.at[2, i], (p, left, t)) for i, x in enumerate((wa, wc))]
    for copy in (to_right[0], to_left[1], to_right[1], to_left[0]):
        copy.start()

    for i in range(HEADS):
        lamt[t, pl.ds(i, 1), :] = jnp.full((1, TOK), lam[i], F32)
    lam_copy = remote(lamt.at[t], lamt.at[t], l_s, l_r, (p, f, 1 - t))
    lam_copy.start()

    cum = scan_lanes(log_sigmoid(gf[...]), jnp.add, 0.0)
    u = gi[...] - cum
    run = scan_lanes(u, jnp.maximum, NEG)
    cum_s[...] = cum
    u_s[...] = u
    m_s[...] = run
    half = iota((1, 128), 1) < 64
    decay = jnp.broadcast_to(cum[:, TOK - 1 : TOK], (HEADS, 128))
    largest = decay + run[:, TOK - 1 : TOK]
    for k in range(4):
        hdr[k : k + 1, :] = jnp.where(half, decay[2 * k : 2 * k + 1], decay[2 * k + 1 : 2 * k + 2])
        hdr[4 + k : 5 + k, :] = jnp.where(half, largest[2 * k : 2 * k + 1], largest[2 * k + 1 : 2 * k + 2])
    st_out[:, 0:8, :] = jnp.broadcast_to(hdr[...][None], (NSP, 8, 128))
    for src, dst, sem in locals_[:3]:
        pltpu.make_async_copy(src, dst, sem).wait()

    def down(h):
        return jnp.transpose(jnp.broadcast_to(u_s[pl.ds(h, 1), :], (128, TOK)))

    def q_half(pair, which):
        q = cqs[:, cols(pair)] * jnp.asarray(0.125, BF16)
        lane = iota((TOK, 128), 1)
        keep = lane < 64 if which == 0 else lane >= 64
        return jnp.where(keep, q, jnp.zeros_like(q))

    def cell_state(k, _):
        expo = []
        for i in range(2):
            h = 2 * k + i
            expo.append(down(h) - m_s[pl.ds(h, 1), :][:, TOK - 1 : TOK])
            cvt[h] = jnp.transpose(cvs[:, cols(h)].astype(F32)).astype(BF16)
        scaled = jnp.exp(jnp.where(half, expo[0], expo[1]))
        weighted = (scaled * cks[:, cols(k)].astype(F32)).astype(BF16)
        state = jnp.where(half, dot_nn(cvt[2 * k], weighted), dot_nn(cvt[2 * k + 1], weighted))
        st_out[:, pl.ds(pl.multiple_of(8 + 8 * k, 8), 8), :] = state.reshape(NSP, 8, 128)
        return 0

    lax.fori_loop(0, 4, cell_state, 0)

    def send_state(i, _):
        to = lax.rem(p + i, NSP)
        remote(st_out.at[to], st_in.at[p], st_s.at[to], st_r.at[p], (to, f, t)).start()
        return 0

    lax.fori_loop(1, NSP, send_state, 0)
    st_in[p] = st_out[p]

    def cell_inside(k, _):
        keys = cks[:, cols(k)]
        causal = iota((TOK, TOK), 0) <= iota((TOK, TOK), 1)
        for i in range(2):
            h = 2 * k + i
            scores = dot_nt(keys, q_half(k, i))
            rows = down(h)
            diff = jnp.concatenate([rows, rows], axis=1) - m_s[pl.ds(h, 1), :]
            weight = (jnp.exp(jnp.where(causal, diff, NEG)) * scores).astype(BF16)
            intra[h] = dot_nn(cvt[h], weight)
        return 0

    lax.fori_loop(0, 4, cell_inside, 0)

    def wait_state(i, _):
        b = lax.rem(p + i, NSP)
        arrived(st_in.at[b], st_r.at[b])
        return 0

    lax.fori_loop(1, NSP, wait_state, 0)

    def advance(b, carry):
        stab, states = carry
        pv_out[b, 0:4, :] = stab
        decays, tops = st_in[b, 0:4, :], st_in[b, 4:8, :]
        new = jnp.maximum(decays + stab, tops)
        keep, take = jnp.exp(decays + stab - new), jnp.exp(tops - new)
        after = []
        for k in range(4):
            at = slice(8 + 8 * k, 16 + 8 * k)
            pv_out[b, at, :] = states[k]
            after.append(keep[k : k + 1] * states[k] + take[k : k + 1] * st_in[b, at, :])
        return new, tuple(after)

    zero = jnp.zeros((8, 128), F32)
    pv_out[:, 4:8, :] = jnp.zeros((NSP, 4, 128), F32)
    lax.fori_loop(0, NSP, advance, (jnp.zeros((4, 128), F32), (zero,) * 4))

    def send_prev(i, _):
        to = lax.rem(p + i, NSP)
        remote(pv_out.at[to], pv_in.at[p], pv_s.at[to], pv_r.at[p], (to, f, t)).start()
        return 0

    lax.fori_loop(1, NSP, send_prev, 0)
    pv_in[p] = pv_out[p]

    arrived(lamt.at[1 - t], l_r)

    def attend(s, _):
        mine = 2 * s + lax.rem(s + t, 2)
        other = 2 * s + lax.rem(s + t + 1, 2)
        for ref, recv, send in ((kb, k_r, rk_s), (vb, v_r, rv_s)):
            block = kv_at(ref, mine)
            arrived(block, recv.at[mine])
            remote(block, block, send.at[s], recv.at[mine], (p, f, 1 - t)).start()
        arrived(qb.at[s], q_r.at[s])
        for ref, recv in ((kb, k_r), (vb, v_r)):
            arrived(kv_at(ref, other), recv.at[other])
        vt[s] = jnp.transpose(vb[s].astype(F32)).astype(BF16)
        q = qb[s] * jnp.asarray(0.125, BF16)
        lane = iota((TOK, 128), 1)
        none = jnp.zeros_like(q)
        maps = (jnp.where(lane < 64, q, none), jnp.where(lane >= 64, q, none))
        mx[...] = jnp.full(mx.shape, NEG, F32)

        def score(kt, masked):
            keys = kb[kt]
            for c in range(2):
                sc = dot_nt(keys, maps[c])
                if masked:
                    seen = iota(sc.shape, 0) <= iota(sc.shape, 1) + (mine - 2 * s) * TOK
                    sc = jnp.where(seen, sc, NEG)
                sbuf[c, kt] = sc
                mx[c] = jnp.maximum(mx[c], jnp.max(sc.reshape(64, 8, TOK), axis=0))

        def score_one(kt, _):
            score(kt, False)
            return 0

        lax.fori_loop(0, s, score_one, 0)
        score(s, True)
        tops = [jnp.max(mx[c], axis=0, keepdims=True) for c in range(2)]
        ls[...] = jnp.zeros(ls.shape, F32)
        acc[...] = jnp.zeros(acc.shape, F32)

        def weigh(kt, _):
            for c in range(2):
                expd = jnp.exp(sbuf[c, kt] - tops[c])
                ls[c] += jnp.sum(expd.reshape(64, 8, TOK), axis=0)
                acc[c] += dot_nn(vt[kt], expd.astype(BF16))
            return 0

        lax.fori_loop(0, s + 1, weigh, 0)
        ratio = [acc[c] / jnp.sum(ls[c], axis=0, keepdims=True) for c in range(2)]
        mixed = ratio[0] - lamt[group, pl.ds(row, 1), :] * ratio[1]
        factor = lax.rsqrt(jnp.mean(mixed * mixed, axis=0, keepdims=True) + EPS) * 0.8
        aout[s] = jnp.transpose(mixed * factor).astype(BF16)
        home = jnp.logical_and(mine == p, group == t)

        @pl.when(jnp.logical_not(home))
        def _():
            remote(aout.at[s], acta.at[:, cols(row)], as_.at[s], ar.at[row], (mine, f, group)).start()

        @pl.when(home)
        def _():
            acta[:, cols(row)] = aout[s]

        return 0

    lax.fori_loop(0, HEADS, attend, 0)

    arrived(w.at[left, 0], w_r.at[1, 0])
    on_right = remote(w.at[left, 0], w.at[left, 0], w_s.at[4], w_r.at[3, 0], (p, right, t))
    on_right.start()
    arrived(w.at[right, 1], w_r.at[2, 1])
    on_left = remote(w.at[right, 1], w.at[right, 1], w_s.at[5], w_r.at[3, 1], (p, left, t))
    on_left.start()

    def wait_prev(i, _):
        b = lax.rem(p + i, NSP)
        arrived(pv_in.at[b], pv_r.at[b])
        return 0

    lax.fori_loop(1, NSP, wait_prev, 0)

    def cell_out(k, _):
        state = pv_in[:, pl.ds(pl.multiple_of(8 + 8 * k, 8), 8), :].reshape(128, 128)
        high = state.astype(BF16)
        low = (state - high.astype(F32)).astype(BF16)
        before = pv_in[0, pl.ds(k, 1), :]
        for i in range(2):
            h = 2 * k + i
            q = q_half(k, i)
            carried = dot_nt(high, q) + dot_nt(low, q)
            cum_h = cum_s[pl.ds(h, 1), :]
            inside = cum_h + m_s[pl.ds(h, 1), :]
            inter = cum_h + before[:, 64 * i : 64 * i + 1]
            stab = jnp.maximum(inside, inter)
            hidden = jnp.exp(inside - stab) * intra[h] + jnp.exp(inter - stab) * carried
            factor = lax.rsqrt(jnp.mean(hidden * hidden, axis=0, keepdims=True) + EPS)
            actc[:, cols(h)] = jnp.transpose(hidden * factor).astype(BF16)
        return 0

    lax.fori_loop(0, 4, cell_out, 0)

    def wait_attn(j, _):
        here = jnp.logical_and(HEADS * t + j == p, owner == t)

        @pl.when(jnp.logical_not(here))
        def _():
            arrived(acta.at[:, cols(j)], ar.at[j])

        return 0

    lax.fori_loop(0, HEADS, wait_attn, 0)

    def rows_of(core):
        return pl.ds(pl.multiple_of(core * 128, 128), 128)

    for i, block in enumerate((f, left, right, across)):
        for k in range(2):
            if (i, k) not in ((1, 0), (2, 1)):
                arrived(w.at[block, k], w_r.at[i, k])

        def product(core):
            return dot_nn(acta[rows_of(core), :], w[block, 0]) + dot_nn(actc[rows_of(core), :], w[block, 1])

        part[i] = product(1 - t).astype(BF16)
        remote(part.at[i], got.at[i], p_s.at[i], p_r.at[i], (p, f, 1 - t)).start()
        own[i] = product(t).astype(BF16)
    for i, block in enumerate((f, left, right, across)):
        arrived(got.at[i], p_r.at[i])
        total = own[i].astype(F32) + got[i].astype(F32)
        out[:, pl.ds(pl.multiple_of(block * 512, 512), 512)] = total.astype(BF16)

    def drain_heads(j, _):
        here = jnp.logical_and(HEADS * t + j == p, t == owner)

        @pl.when(jnp.logical_not(here))
        def _():
            sent(ak.at[:, cols(j)], k_s.at[j])
            sent(av.at[:, cols(j)], v_s.at[j])
            sent(aq.at[:, cols(j)], q_s.at[j])

        mine = 2 * j + lax.rem(j + t, 2)
        sent(kv_at(kb, mine), rk_s.at[j])
        sent(kv_at(vb, mine), rv_s.at[j])

        @pl.when(jnp.logical_not(jnp.logical_and(mine == p, group == t)))
        def _():
            sent(aout.at[j], as_.at[j])

        return 0

    lax.fori_loop(0, HEADS, drain_heads, 0)

    def drain_states(i, _):
        to = lax.rem(p + i, NSP)
        sent(st_out.at[to], st_s.at[to])
        sent(pv_out.at[to], pv_s.at[to])
        return 0

    lax.fori_loop(1, NSP, drain_states, 0)
    for copy in (*to_right, *to_left, on_right, on_left, lam_copy):
        copy.wait_send()
    for i in range(4):
        sent(part.at[i], p_s.at[i])


def per_device(aq, ak, av, lam, cq, ck, cv, gi, gf, wa, wc):
    dma = pltpu.SemaphoreType.DMA
    scratch = [
        pltpu.VMEM((8, 512, 128), BF16),
        pltpu.VMEM((8, 512, 128), BF16),
        pltpu.VMEM((8, 128, 512), BF16),
        pltpu.VMEM((8, TOK, 128), BF16),
        pltpu.VMEM((2, 8, 512, TOK), F32),
        pltpu.VMEM((2, 8, TOK), F32),
        pltpu.VMEM((2, 8, TOK), F32),
        pltpu.VMEM((2, 128, TOK), F32),
        pltpu.VMEM((8, TOK, 128), BF16),
        pltpu.VMEM((TOK, 1024), BF16),
        pltpu.VMEM((TOK, 1024), BF16),
        pltpu.VMEM((NFS, 2, 1024, 512), BF16),
        pltpu.VMEM((NFS, 128, 512), BF16),
        pltpu.VMEM((NFS, 128, 512), BF16),
        pltpu.VMEM((NFS, 128, 512), BF16),
        pltpu.VMEM((TOK, 512), BF16),
        pltpu.VMEM((TOK, 512), BF16),
        pltpu.VMEM((TOK, 1024), BF16),
        pltpu.VMEM((HEADS, 128, TOK), F32),
        pltpu.VMEM((HEADS, 128, TOK), BF16),
        pltpu.VMEM((8, 128), F32),
        pltpu.VMEM((NSP, 40, 128), F32),
        pltpu.VMEM((NSP, 40, 128), F32),
        pltpu.VMEM((NSP, 40, 128), F32),
        pltpu.VMEM((NSP, 40, 128), F32),
        pltpu.VMEM((HEADS, TOK), F32),
        pltpu.VMEM((HEADS, TOK), F32),
        pltpu.VMEM((HEADS, TOK), F32),
        pltpu.VMEM((2, HEADS, TOK), F32),
        dma((8,)), dma((8,)), dma((8,)),
        dma((16,)), dma((16,)), dma((8,)),
        dma((8,)), dma((8,)),
        dma((8,)), dma((8,)),
        dma((6,)), dma((4, 2)),
        dma((4,)), dma((4,)),
        dma((16,)), dma((16,)), dma((16,)), dma((16,)),
        dma((3,)), dma(()), dma(()),
    ]
    hbm = pl.BlockSpec(memory_space=pl.ANY)
    vmem = pl.BlockSpec(memory_space=pltpu.VMEM)
    smem = pl.BlockSpec(memory_space=pltpu.SMEM)
    y = pl.pallas_call(
        kernel,
        out_shape=jax.ShapeDtypeStruct((128, 2048), BF16),
        in_specs=[hbm, hbm, hbm, smem, hbm, hbm, hbm, vmem, vmem, hbm, hbm],
        out_specs=vmem,
        scratch_shapes=scratch,
        compiler_params=pltpu.CompilerParams(
            collective_id=0, has_side_effects=True, vmem_limit_bytes=56 * 1024 * 1024
        ),
    )(aq[0], ak[0], av[0], lam, cq[0], ck[0], cv[0], gi[0], gf[0], wa, wc)
    return y[None]


def solution(mesh):
    placed = (
        P("fs", "sp", "tp"),
        P("fs", "sp", "tp"),
        P("fs", "sp", "tp"),
        P("tp"),
        P("fs", "sp", "tp"),
        P("fs", "sp", "tp"),
        P("fs", "sp", "tp"),
        P("fs", "tp", "sp"),
        P("fs", "tp", "sp"),
        P("tp", "fs"),
        P("tp", "fs"),
    )
    return jax.shard_map(
        per_device,
        mesh=mesh,
        in_specs=placed,
        out_specs=P("fs", ("sp", "tp"), None),
        check_vma=False,
    )
```

time: 381 us -> 98.3 us (0.26)
  the two profiles are of different devices: /device:TPU:97 before, /device:TPU:1 now
where the time goes in v1:
time: 98.3 us; the launch traced here: 98.1 us
  Pallas kernels  96.2 us (98%)
  local copies, waits for them, and re-layouts  1.88 us (2%)
    pallas_call x1, Pallas kernels, per_device(): pl.pallas_call(kernel, out_shape=jax.ShapeDtypeStruct((128, 2048), BF16),...  96.2 us

profile of v1, /device:TPU:1, one launch (start us, length us, event | category | flops | bytes accessed | tf_op | source)
XLA Modules:
  0.0 98.1 jit_solution(2553068229487010307)
XLA Ops:
  0.0 96.2 %shard_map.109 = bf16[128,2048]{1,0:T(8,128)(2,1)} custom-call(bf16[256,1024]{1,0:T(8,128)(2,1)} %bitcast.10, bf16[256,1024]{1,0:T(8,128)(2,1)} %bitcast.11, bf16[256,1024]{1,0:T(8,128)(2,1)} %bitcast.12, f32[8]{0:T(128)} %lam.1, bf16[256,512]{1,0:T(8,128)(2,1)} %bitcast.14, bf16[256,512]{1,0:T(8,128)(2,1)} %bitcast.15, bf16[256,1024]{1,0:T(8,128)(2,1)} %bitcast.13, ...), custom_call_target="tpu_custom_call" | custom-call | tf_op jit(solution)/shard_map/pallas_call | solution.py:435
  96.2 1.9 %copy.13 = bf16[1,128,2048]{2,1,0:T(8,128)(2,1)} copy(bf16[1,128,2048]{2,1,0:T(8,128)(2,1)} %bitcast.9) | data formatting | bytes 1048576

commit v2 on v1

--- a/solution.py
+++ b/solution.py
@@ -53,7 +53,7 @@
     kb, vb, vt, qb, sbuf, mx, ls, acc, aout, acta, actc, w, part, own, got,
     cqs, cks, cvs, intra, cvt, hdr, st_out, st_in, pv_out, pv_in, cum_s, u_s, m_s, lamt,
     k_s, v_s, q_s, k_r, v_r, q_r, rk_s, rv_s, as_, ar, w_s, w_r, p_s, p_r,
-    st_s, st_r, pv_s, pv_r, c_r, l_s, l_r,
+    st_s, st_r, pv_s, pv_r, c_r, l_s, l_r, f_s, f_r, b_s, b_r,
 ):
     p = lax.axis_index("sp")
     f = lax.axis_index("fs")
@@ -87,10 +87,11 @@
         pl.semaphore_signal(barrier, inc=1, device_id=(peer // 2, f, lax.rem(peer, 2)), device_id_type=MESH)
         return 0
 
-    lax.fori_loop(1, 2 * NSP, greet, 0)
-    for side in (left, right):
-        pl.semaphore_signal(barrier, inc=1, device_id=(p, side, t), device_id_type=MESH)
-    pl.semaphore_wait(barrier, 2 * NSP + 1)
+    with jax.named_scope("barrier"):
+        lax.fori_loop(1, 2 * NSP, greet, 0)
+        for side in (left, right, across):
+            pl.semaphore_signal(barrier, inc=1, device_id=(p, side, t), device_id_type=MESH)
+        pl.semaphore_wait(barrier, 2 * NSP + 2)
 
     locals_ = (
         (cq, cqs, c_r.at[0]), (ck, cks, c_r.at[1]), (cv, cvs, c_r.at[2]),
@@ -120,12 +121,33 @@
 
         return 0
 
-    lax.fori_loop(0, HEADS, send_heads, 0)
-
-    to_right = [remote(x, w.at[f, i], w_s.at[i], w_r.at[1, i], (p, right, t)) for i, x in enumerate((wa, wc))]
-    to_left = [remote(x, w.at[f, i], w_s.at[2 + i], w_r.at[2, i], (p, left, t)) for i, x in enumerate((wa, wc))]
-    for copy in (to_right[0], to_left[1], to_right[1], to_left[0]):
+    with jax.named_scope("send_heads"):
+        lax.fori_loop(0, HEADS, send_heads, 0)
+
+    z, y = p // 4, lax.rem(p, 4)
+    pieces = (
+        pl.ds(pl.multiple_of(y * 128, 128), 128),
+        pl.ds(pl.multiple_of(512 + z * 128, 128), 128),
+    )
+    first = []
+    for i, to in ((1, right), (2, left), (3, across)):
+        for k, rows in enumerate(pieces):
+            first.append(remote(wa.at[rows], w.at[f, 0, rows], f_s.at[i - 1, k], f_r.at[i - 1, k], (p, to, t)))
+    halves = (pl.ds(0, 512), pl.ds(512, 512))
+    to_right = [remote(wc.at[rows], w.at[f, 1, rows], w_s.at[k], w_r.at[1, k], (p, right, t)) for k, rows in enumerate(halves)]
+    to_left = [remote(wc.at[rows], w.at[f, 1, rows], w_s.at[2 + k], w_r.at[2, k], (p, left, t)) for k, rows in enumerate(halves)]
+    for copy in (*first, to_right[0], to_left[1], to_right[1], to_left[0]):
         copy.start()
+
+    def along(axis, d):
+        return (z * 4 + lax.rem(y + d, 4), f, t) if axis == 0 else (lax.rem(z + d, 4) * 4 + y, f, t)
+
+    def fan_out(i, block):
+        for k, rows in enumerate(pieces):
+            piece = w.at[block, 0, rows]
+            arrived(piece, f_r.at[i, k])
+            for d in (1, 2, 3):
+                remote(piece, piece, b_s.at[i, k, d - 1], b_r.at[i, k, (y, z)[k]], along(k, d)).start()
 
     for i in range(HEADS):
         lamt[t, pl.ds(i, 1), :] = jnp.full((1, TOK), lam[i], F32)
@@ -169,7 +191,8 @@
         st_out[:, pl.ds(pl.multiple_of(8 + 8 * k, 8), 8), :] = state.reshape(NSP, 8, 128)
         return 0
 
-    lax.fori_loop(0, 4, cell_state, 0)
+    with jax.named_scope("cell_state"):
+        lax.fori_loop(0, 4, cell_state, 0)
 
     def send_state(i, _):
         to = lax.rem(p + i, NSP)
@@ -178,6 +201,9 @@
 
     lax.fori_loop(1, NSP, send_state, 0)
     st_in[p] = st_out[p]
+    with jax.named_scope("fan_out"):
+        fan_out(0, left)
+        fan_out(1, right)
 
     def cell_inside(k, _):
         keys = cks[:, cols(k)]
@@ -191,52 +217,82 @@
             intra[h] = dot_nn(cvt[h], weight)
         return 0
 
-    lax.fori_loop(0, 4, cell_inside, 0)
-
-    def wait_state(i, _):
-        b = lax.rem(p + i, NSP)
-        arrived(st_in.at[b], st_r.at[b])
-        return 0
-
-    lax.fori_loop(1, NSP, wait_state, 0)
-
-    def advance(b, carry):
-        stab, states = carry
-        pv_out[b, 0:4, :] = stab
-        decays, tops = st_in[b, 0:4, :], st_in[b, 4:8, :]
-        new = jnp.maximum(decays + stab, tops)
-        keep, take = jnp.exp(decays + stab - new), jnp.exp(tops - new)
-        after = []
-        for k in range(4):
-            at = slice(8 + 8 * k, 16 + 8 * k)
-            pv_out[b, at, :] = states[k]
-            after.append(keep[k : k + 1] * states[k] + take[k : k + 1] * st_in[b, at, :])
-        return new, tuple(after)
-
-    zero = jnp.zeros((8, 128), F32)
-    pv_out[:, 4:8, :] = jnp.zeros((NSP, 4, 128), F32)
-    lax.fori_loop(0, NSP, advance, (jnp.zeros((4, 128), F32), (zero,) * 4))
-
-    def send_prev(i, _):
-        to = lax.rem(p + i, NSP)
-        remote(pv_out.at[to], pv_in.at[p], pv_s.at[to], pv_r.at[p], (to, f, t)).start()
-        return 0
-
-    lax.fori_loop(1, NSP, send_prev, 0)
-    pv_in[p] = pv_out[p]
+    with jax.named_scope("cell_inside"):
+        lax.fori_loop(0, 4, cell_inside, 0)
+
+    with jax.named_scope("fan_out"):
+        fan_out(2, across)
+
+    def scan_states():
+        def wait_state(i, _):
+            b = lax.rem(p + i, NSP)
+            arrived(st_in.at[b], st_r.at[b])
+            return 0
+
+        with jax.named_scope("wait_state"):
+            lax.fori_loop(1, NSP, wait_state, 0)
+
+        def advance(b, carry):
+            stab, states = carry
+            pv_out[b, 0:4, :] = stab
+            decays, tops = st_in[b, 0:4, :], st_in[b, 4:8, :]
+            new = jnp.maximum(decays + stab, tops)
+            keep, take = jnp.exp(decays + stab - new), jnp.exp(tops - new)
+            after = []
+            for k in range(4):
+                at = slice(8 + 8 * k, 16 + 8 * k)
+                pv_out[b, at, :] = states[k]
+                after.append(keep[k : k + 1] * states[k] + take[k : k + 1] * st_in[b, at, :])
+            return new, tuple(after)
+
+        zero = jnp.zeros((8, 128), F32)
+        pv_out[:, 4:8, :] = jnp.zeros((NSP, 4, 128), F32)
+        with jax.named_scope("advance"):
+            lax.fori_loop(0, NSP, advance, (jnp.zeros((4, 128), F32), (zero,) * 4))
+
+        def send_prev(i, _):
+            to = lax.rem(p + i, NSP)
+            remote(pv_out.at[to], pv_in.at[p], pv_s.at[to], pv_r.at[p], (to, f, t)).start()
+            return 0
+
+        lax.fori_loop(1, NSP, send_prev, 0)
+        pv_in[p] = pv_out[p]
+
+    on_right = remote(w.at[left, 1, halves[0]], w.at[left, 1, halves[0]], w_s.at[4], w_r.at[3, 0], (p, right, t))
+    on_left = remote(w.at[right, 1, halves[1]], w.at[right, 1, halves[1]], w_s.at[5], w_r.at[3, 1], (p, left, t))
+
+    def forward():
+        with jax.named_scope("wait_ring"):
+            arrived(w.at[left, 1, halves[0]], w_r.at[1, 0])
+        on_right.start()
+        with jax.named_scope("wait_ring"):
+            arrived(w.at[right, 1, halves[1]], w_r.at[2, 1])
+        on_left.start()
+
+    def pass_on(s):
+        mine = 2 * s + lax.rem(s + t, 2)
+        for ref, recv, send in ((kb, k_r, rk_s), (vb, v_r, rv_s)):
+            block = kv_at(ref, mine)
+            with jax.named_scope("wait_mine"):
+                arrived(block, recv.at[mine])
+            remote(block, block, send.at[s], recv.at[mine], (p, f, 1 - t)).start()
 
     arrived(lamt.at[1 - t], l_r)
 
     def attend(s, _):
         mine = 2 * s + lax.rem(s + t, 2)
         other = 2 * s + lax.rem(s + t + 1, 2)
-        for ref, recv, send in ((kb, k_r, rk_s), (vb, v_r, rv_s)):
-            block = kv_at(ref, mine)
-            arrived(block, recv.at[mine])
-            remote(block, block, send.at[s], recv.at[mine], (p, f, 1 - t)).start()
-        arrived(qb.at[s], q_r.at[s])
-        for ref, recv in ((kb, k_r), (vb, v_r)):
-            arrived(kv_at(ref, other), recv.at[other])
+
+        @pl.when(s + 2 < HEADS)
+        def _():
+            pass_on(s + 2)
+
+        pl.when(s == 4)(scan_states)
+        pl.when(s == 5)(forward)
+        with jax.named_scope("wait_other"):
+            arrived(qb.at[s], q_r.at[s])
+            for ref, recv in ((kb, k_r), (vb, v_r)):
+                arrived(kv_at(ref, other), recv.at[other])
         vt[s] = jnp.transpose(vb[s].astype(F32)).astype(BF16)
         q = qb[s] * jnp.asarray(0.125, BF16)
         lane = iota((TOK, 128), 1)
@@ -258,8 +314,9 @@
             score(kt, False)
             return 0
 
-        lax.fori_loop(0, s, score_one, 0)
-        score(s, True)
+        with jax.named_scope("score"):
+            lax.fori_loop(0, s, score_one, 0)
+            score(s, True)
         tops = [jnp.max(mx[c], axis=0, keepdims=True) for c in range(2)]
         ls[...] = jnp.zeros(ls.shape, F32)
         acc[...] = jnp.zeros(acc.shape, F32)
@@ -271,7 +328,8 @@
                 acc[c] += dot_nn(vt[kt], expd.astype(BF16))
             return 0
 
-        lax.fori_loop(0, s + 1, weigh, 0)
+        with jax.named_scope("weigh"):
+            lax.fori_loop(0, s + 1, weigh, 0)
         ratio = [acc[c] / jnp.sum(ls[c], axis=0, keepdims=True) for c in range(2)]
         mixed = ratio[0] - lamt[group, pl.ds(row, 1), :] * ratio[1]
         factor = lax.rsqrt(jnp.mean(mixed * mixed, axis=0, keepdims=True) + EPS) * 0.8
@@ -288,21 +346,18 @@
 
         return 0
 
-    lax.fori_loop(0, HEADS, attend, 0)
-
-    arrived(w.at[left, 0], w_r.at[1, 0])
-    on_right = remote(w.at[left, 0], w.at[left, 0], w_s.at[4], w_r.at[3, 0], (p, right, t))
-    on_right.start()
-    arrived(w.at[right, 1], w_r.at[2, 1])
-    on_left = remote(w.at[right, 1], w.at[right, 1], w_s.at[5], w_r.at[3, 1], (p, left, t))
-    on_left.start()
+    pass_on(0)
+    pass_on(1)
+    with jax.named_scope("attend"):
+        lax.fori_loop(0, HEADS, attend, 0)
 
     def wait_prev(i, _):
         b = lax.rem(p + i, NSP)
         arrived(pv_in.at[b], pv_r.at[b])
         return 0
 
-    lax.fori_loop(1, NSP, wait_prev, 0)
+    with jax.named_scope("wait_prev"):
+        lax.fori_loop(1, NSP, wait_prev, 0)
 
     def cell_out(k, _):
         state = pv_in[:, pl.ds(pl.multiple_of(8 + 8 * k, 8), 8), :].reshape(128, 128)
@@ -322,7 +377,8 @@
             actc[:, cols(h)] = jnp.transpose(hidden * factor).astype(BF16)
         return 0
 
-    lax.fori_loop(0, 4, cell_out, 0)
+    with jax.named_scope("cell_out"):
+        lax.fori_loop(0, 4, cell_out, 0)
 
     def wait_attn(j, _):
         here = jnp.logical_and(HEADS * t + j == p, owner == t)
@@ -333,15 +389,26 @@
 
         return 0
 
-    lax.fori_loop(0, HEADS, wait_attn, 0)
+    with jax.named_scope("wait_attn"):
+        lax.fori_loop(0, HEADS, wait_attn, 0)
 
     def rows_of(core):
         return pl.ds(pl.multiple_of(core * 128, 128), 128)
 
     for i, block in enumerate((f, left, right, across)):
-        for k in range(2):
-            if (i, k) not in ((1, 0), (2, 1)):
-                arrived(w.at[block, k], w_r.at[i, k])
+        with jax.named_scope("wait_rows"):
+            if i == 0:
+                arrived(w.at[block, 0], w_r.at[0, 0])
+                arrived(w.at[block, 1], w_r.at[0, 1])
+            else:
+                for k in range(2):
+                    if (i, k) not in ((1, 0), (2, 1)):
+                        arrived(w.at[block, 1, halves[k]], w_r.at[i, k])
+                for k, own_at in enumerate((y, z)):
+                    for d in (1, 2, 3):
+                        at = lax.rem(own_at + d, 4)
+                        rows = pl.ds(pl.multiple_of(512 * k + at * 128, 128), 128)
+                        arrived(w.at[block, 0, rows], b_r.at[i - 1, k, at])
 
         def product(core):
             return dot_nn(acta[rows_of(core), :], w[block, 0]) + dot_nn(actc[rows_of(core), :], w[block, 1])
@@ -350,7 +417,8 @@
         remote(part.at[i], got.at[i], p_s.at[i], p_r.at[i], (p, f, 1 - t)).start()
         own[i] = product(t).astype(BF16)
     for i, block in enumerate((f, left, right, across)):
-        arrived(got.at[i], p_r.at[i])
+        with jax.named_scope("wait_got"):
+            arrived(got.at[i], p_r.at[i])
         total = own[i].astype(F32) + got[i].astype(F32)
         out[:, pl.ds(pl.multiple_of(block * 512, 512), 512)] = total.astype(BF16)
 
@@ -373,7 +441,8 @@
 
         return 0
 
-    lax.fori_loop(0, HEADS, drain_heads, 0)
+    with jax.named_scope("drain"):
+        lax.fori_loop(0, HEADS, drain_heads, 0)
 
     def drain_states(i, _):
         to = lax.rem(p + i, NSP)
@@ -382,8 +451,12 @@
         return 0
 
     lax.fori_loop(1, NSP, drain_states, 0)
-    for copy in (*to_right, *to_left, on_right, on_left, lam_copy):
+    for copy in (*first, *to_right, *to_left, on_right, on_left, lam_copy):
         copy.wait_send()
+    for i, block in enumerate((left, right, across)):
+        for k, rows in enumerate(pieces):
+            for d in range(3):
+                sent(w.at[block, 0, rows], b_s.at[i, k, d])
     for i in range(4):
         sent(part.at[i], p_s.at[i])
 
@@ -428,6 +501,7 @@
         dma((4,)), dma((4,)),
         dma((16,)), dma((16,)), dma((16,)), dma((16,)),
         dma((3,)), dma(()), dma(()),
+        dma((3, 2)), dma((3, 2)), dma((3, 2, 3)), dma((3, 2, 4)),
     ]
     hbm = pl.BlockSpec(memory_space=pl.ANY)
     vmem = pl.BlockSpec(memory_space=pltpu.VMEM)

time: 98.3 us -> 71.7 us (0.73)
  Pallas kernels: 96.2 us -> 69.6 us
    pallas_call x1, Pallas kernels: 96.2 us -> 69.6 us  [per_device(): pl.pallas_call(kernel, out_shape=jax.ShapeDtypeStruct((128, 2048), BF16),...]
where the time goes in v2:
time: 71.7 us; the launch traced here: 71.5 us
  Pallas kernels  69.6 us (97%)
  local copies, waits for them, and re-layouts  1.88 us (3%)
    pallas_call x1, Pallas kernels, per_device(): pl.pallas_call(kernel, out_shape=jax.ShapeDtypeStruct((128, 2048), BF16),...  69.6 us
    unnamed x1, local copies, waits for them, and re-layouts  1.88 us

profile of v2, /device:TPU:1, one launch (start us, length us, event | category | flops | bytes accessed | tf_op | source)
XLA Modules:
  0.0 71.5 jit_solution(6415117522535092711)
XLA Ops:
  0.0 69.6 %shard_map.109 = bf16[128,2048]{1,0:T(8,128)(2,1)} custom-call(bf16[256,1024]{1,0:T(8,128)(2,1)} %bitcast.10, bf16[256,1024]{1,0:T(8,128)(2,1)} %bitcast.11, bf16[256,1024]{1,0:T(8,128)(2,1)} %bitcast.12, f32[8]{0:T(128)} %lam.1, bf16[256,512]{1,0:T(8,128)(2,1)} %bitcast.14, bf16[256,512]{1,0:T(8,128)(2,1)} %bitcast.15, bf16[256,1024]{1,0:T(8,128)(2,1)} %bitcast.13, ...), custom_call_target="tpu_custom_call" | custom-call | tf_op jit(solution)/shard_map/pallas_call | solution.py:509
  69.6 1.9 %copy.13 = bf16[1,128,2048]{2,1,0:T(8,128)(2,1)} copy(bf16[1,128,2048]{2,1,0:T(8,128)(2,1)} %bitcast.9) | data formatting | bytes 1048576
